TPU v7x, 256 devices: a whole 4x4x8 slice. The times are simulated.
256 devices in a mesh: sp: 64 (over z, y, core), tp: 4 (over x).
Axes of the slice: x: 4, y: 4, z: 8, core: 2. Of those that a mesh axis runs over, the one named last changes fastest.
Arguments:
- moe_input: bfloat16 [8192, 2048], P('sp', 'tp'), may hold values from -6 to 6
- cotangent: bfloat16 [8192, 2048], P('sp', 'tp'), may hold values from -16 to 16
- expert_ids: int32 [8192, 2], P('sp'), may hold values from 0 to 63, as said below
- routing_weights: float32 [8192, 2], P('sp'), may hold values from 0.1 to 0.6
- gate_weight: bfloat16 [64, 2048, 1024], P('sp', None, 'tp'), may hold values from -0.125 to 0.125
- up_weight: bfloat16 [64, 2048, 1024], P('sp', None, 'tp'), may hold values from -0.125 to 0.125
- down_weight: bfloat16 [64, 1024, 2048], P('sp', 'tp'), may hold values from -0.1875 to 0.1875
- inner_x: bfloat16 [8192, 4096], P('sp', 'tp'), may hold values from -6 to 6
- inner_b: bfloat16 [8192, 256], P('sp', 'tp'), may hold values from -6 to 6
- inner_c: bfloat16 [8192, 256], P('sp', 'tp'), may hold values from -6 to 6
- gate_z: bfloat16 [8192, 4096], P('sp', 'tp'), may hold values from -6 to 6
- step_raw: float32 [8192, 64], P('sp', 'tp'), may hold values from -30 to 2
- decay_rate: float32 [64], P('tp'), may hold values from 1 to 16
- skip_weight: float32 [64], P('tp'), may hold values from 0.1 to 1.9
- norm_gain: float32 [4096], P('tp'), may hold values from 0.1 to 1.9
- w_out: bfloat16 [2048, 4096], P(None, 'tp'), may hold values from -0.09375 to 0.09375
Outputs:
- gate_weight_gradient: bfloat16 [64, 2048, 1024], P('sp', None, 'tp')
- up_weight_gradient: bfloat16 [64, 2048, 1024], P('sp', None, 'tp')
- down_weight_gradient: bfloat16 [64, 1024, 2048], P('sp', 'tp')
- grad_out: float32 [2048, 4096], P('sp', 'tp')
- grad_inner_x: bfloat16 [8192, 4096], P('sp', 'tp')
- grad_inner_b: float32 [8192, 256], P('sp', 'tp')
- grad_inner_c: float32 [8192, 256], P('sp', 'tp')
- grad_gate_z: bfloat16 [8192, 4096], P('sp', 'tp')
- grad_step_raw: float32 [8192, 64], P('sp', 'tp')
Inputs may be any that keep to these rules, and one draw needn't show every extreme that they name: `expert_ids`: the two entries of a row differ and lie in the same group of 16 consecutive experts. In each aligned block of 128 rows no expert is named more than 8 times; one group of experts, the same for all blocks, takes exactly half of every block's rows, and each of its experts is named exactly 8 times in every block.
All inputs are finite; a program needn't handle non-finite values.
Results may differ from a plain program's by a relative error of at most 0.015.
Values may be sent and summed in bfloat16 or wider, within the bound.
No kernel may reach another device: no remote copies, remote signals or barrier semaphores. Data moves between devices by JAX's collectives and lax.ppermute only.
A program may use at most 128 MiB of HBM per device.

v0:
```python
from functools import partial

import jax
import jax.numpy as jnp
from jax import lax
from jax.sharding import Mesh
from jax.sharding import PartitionSpec as P

HEAD_DIM = 64
STATE = 64
SPAN = 128
SP = ("sp_0", "sp_1", "sp_2")


EPS = 0.01


def sent_together(arrays, axis, split_dim, concat_dim, along):
    both = jnp.concatenate(arrays, axis=along)
    out, at, finished = (
        lax.all_to_all(both, axis, split_axis=split_dim, concat_axis=concat_dim, tiled=True),
        0,
        [],
    )
    for a in arrays:
        finished.append(lax.slice_in_dim(out, at, at + a.shape[along], axis=along))
        at += a.shape[along]
    return tuple(finished)


def in_one_piece(arrays, axis, dim, along):
    both = jnp.concatenate(arrays, axis=along)
    out, at, finished = (lax.all_gather(both, axis, axis=dim, tiled=True), 0, [])
    for a in arrays:
        finished.append(lax.slice_in_dim(out, at, at + a.shape[along], axis=along))
        at += a.shape[along]
    return tuple(finished)


def cut_along(shard, dim, devices):
    before, after = (shard.shape[:dim], shard.shape[dim + 1 :])
    return jnp.moveaxis(shard.reshape(*before, devices, -1, *after), dim, 0)


def sum_at_owner(shard, axis, dim):
    devices = lax.axis_size(axis)
    tiles = lax.all_to_all(cut_along(shard, dim, devices), axis, 0, 0, tiled=True)
    return jnp.sum(tiles.astype(jnp.float32), axis=0)


def from_everyone(shard, axis):
    copies = jnp.broadcast_to(shard, (lax.axis_size(axis), *shard.shape))
    return lax.all_to_all(copies, axis, split_axis=0, concat_axis=0, tiled=True)


def in_order(tiles, dim):
    tiles = jnp.moveaxis(tiles, 0, dim)
    dims = tiles.shape
    return tiles.reshape(*dims[:dim], dims[dim] * dims[dim + 1], *dims[dim + 2 :])


def gathered_copies(shard, axis, dim):
    tiles = from_everyone(shard, axis)
    return in_order(tiles, dim)


def neutral_like(shard, identity):
    return jax.tree.map(
        lambda a, e: jnp.broadcast_to(jnp.asarray(e, a.dtype), a.shape), shard, identity
    )


def prefix_by_axis(shard, axes, combine, identity):
    before = start = neutral_like(shard, identity)
    subtotal = shard
    for axis in reversed(axes):
        devices, mine = (lax.axis_size(axis), lax.axis_index(axis))
        pieces = jax.tree.map(
            lambda part, kind: lax.all_gather(part.astype(kind), axis),
            subtotal,
            (jnp.bfloat16, jnp.bfloat16),
        )
        inside, subtotal = (start, start)
        for k in range(devices):
            passed = k < mine
            subtotal = combine(
                subtotal, jax.tree.map(lambda part, own: part[k].astype(own.dtype), pieces, shard)
            )
            inside = jax.tree.map(lambda new, old: jnp.where(passed, new, old), subtotal, inside)
        before = combine(inside, before)
    return before


def own_rows(subtotal, axes):
    for axis in axes:
        subtotal = lax.psum_scatter(subtotal, axis, scatter_dimension=0, tiled=True)
    return subtotal


def carried_in(shard, axes, combine, identity):
    before = start = neutral_like(shard, identity)
    subtotal = shard
    for axis in reversed(axes):
        devices, mine = (lax.axis_size(axis), lax.axis_index(axis))
        pieces = jax.tree.map(
            lambda part, kind: lax.all_gather(part.astype(kind), axis),
            subtotal,
            jax.tree.map(lambda a: jnp.bfloat16 if a.dtype == jnp.float32 else a.dtype, shard),
        )
        inside, subtotal = (start, start)
        for k in reversed(range(devices)):
            passed = k > mine
            subtotal = combine(
                subtotal, jax.tree.map(lambda part, own: part[k].astype(own.dtype), pieces, shard)
            )
            inside = jax.tree.map(lambda new, old: jnp.where(passed, new, old), subtotal, inside)
        before = combine(inside, before)
    return before


def slot_positions(chosen, expert_list, expert_capacity):
    listed = chosen.reshape(-1)
    onehot = (listed[:, None] == jnp.arange(expert_list, dtype=jnp.int32)[None, :]).astype(
        jnp.int32
    )
    before = jnp.cumsum(onehot, axis=0) - onehot
    return listed * expert_capacity + jnp.sum(before * onehot, axis=1)


def prepare(inner_x32, inner_b32, step_raw, decays):
    tok_rows = inner_x32.shape[0]
    heads = decays.shape[0]
    groups = inner_b32.shape[1] // STATE
    per_group = heads // groups
    blocks = tok_rows // SPAN
    x_act = jax.nn.silu(inner_x32).reshape(tok_rows, heads, HEAD_DIM)
    b_blocks = jax.nn.silu(inner_b32).reshape(blocks, SPAN, groups, STATE)
    step_size = jax.nn.softplus(step_raw)
    decay_log = (-step_size * decays[None, :]).reshape(blocks, SPAN, groups, per_group)
    scaled = (x_act * step_size[:, :, None]).reshape(blocks, SPAN, groups, per_group, HEAD_DIM)
    return (x_act, b_blocks, decay_log, scaled)


def advance(carry_state, block_in):
    x_block, log_block, b_block = block_in
    running = jnp.cumsum(log_block, axis=0)
    to_end = jnp.exp(running[-1] - running)
    fresh_state = jnp.einsum("lgn,lge,lgep->gepn", b_block, to_end, x_block)
    return (carry_state * jnp.exp(running[-1])[:, :, None, None] + fresh_state, None)


def block_outputs(carry_state, block_in):
    x_block, log_block, b_block, c_block = block_in
    span_len = x_block.shape[0]
    running = jnp.cumsum(log_block, axis=0)
    places = jnp.arange(span_len)
    causal = (places[:, None] >= places[None, :])[:, :, None, None]
    between = running[:, None] - running[None, :]
    weights = jnp.where(causal, jnp.exp(jnp.where(causal, between, 0.0)), 0.0)
    scores = jnp.einsum("lgn,sgn->lsg", c_block, b_block)
    inside = jnp.einsum("lsg,lsge,sgep->lgep", scores, weights, x_block)
    carried = jnp.einsum("lgn,gepn,lge->lgep", c_block, carry_state, jnp.exp(running))
    to_end = jnp.exp(running[-1] - running)
    fresh_state = jnp.einsum("lgn,lge,lgep->gepn", b_block, to_end, x_block)
    return (carry_state * jnp.exp(running[-1])[:, :, None, None] + fresh_state, inside + carried)


def mixer_output(
    inner_x32, inner_b32, inner_c32, gate_z32, step_raw, carry_in, decays, skip_weight, norm_gain
):
    tok_rows = inner_x32.shape[0]
    heads = decays.shape[0]
    groups = inner_b32.shape[1] // STATE
    x_act, b_blocks, decay_log, scaled = prepare(inner_x32, inner_b32, step_raw, decays)
    c_blocks = jax.nn.silu(inner_c32).reshape(tok_rows // SPAN, SPAN, groups, STATE)
    outputs = lax.scan(block_outputs, carry_in, (scaled, decay_log, b_blocks, c_blocks))[1]
    mixed_out = outputs.reshape(tok_rows, heads, HEAD_DIM) + x_act * skip_weight[None, :, None]
    gated_out = mixed_out.reshape(tok_rows, heads * HEAD_DIM) * jax.nn.silu(gate_z32)
    grouped = gated_out.reshape(tok_rows, groups, -1)
    normed = grouped * lax.rsqrt(jnp.mean(grouped * grouped, axis=2, keepdims=True) + EPS)
    return normed.reshape(tok_rows, -1) * norm_gain[None, :]


def carry_forward(earlier, latter):
    return (earlier[0] * latter[0], earlier[1] * latter[0][:, :, None, None] + latter[1])


def carry_back(earlier, latter):
    return (latter[0] * earlier[0], latter[1] + latter[0][:, :, None, None] * earlier[1])


def body(
    moe_input,
    cotangent,
    expert_ids,
    routing_weights,
    gate_weight,
    up_weight,
    down_weight,
    inner_x,
    inner_b,
    inner_c,
    gate_z,
    step_raw,
    decay_rate,
    skip_weight,
    norm_gain,
    w_out,
):
    tok_rows, chosen_count = expert_ids.shape
    local_experts = gate_weight.shape[0]
    senders = lax.axis_size(SP)
    expert_list = local_experts * senders
    expert_capacity = 4 * tok_rows // expert_list
    place_into_slots = slot_positions(expert_ids, expert_list, expert_capacity)
    owner = (
        jnp.full((expert_list * expert_capacity,), tok_rows, jnp.int32)
        .at[place_into_slots]
        .set(jnp.arange(tok_rows * chosen_count, dtype=jnp.int32) // chosen_count)
    )
    scaling = (
        jnp.zeros((expert_list * expert_capacity,), jnp.float32)
        .at[place_into_slots]
        .set(routing_weights.reshape(-1))
    )

    def to_slots(source, weighted):
        padded = jnp.concatenate([source, jnp.zeros((1, source.shape[1]), source.dtype)], axis=0)
        picked = padded[owner]
        if weighted:
            picked = (picked.astype(jnp.float32) * scaling[:, None]).astype(jnp.bfloat16)
        return picked.reshape(senders, local_experts, expert_capacity, source.shape[1])

    part_in, part_grad = sent_together(
        (to_slots(moe_input, False), to_slots(cotangent, True)), SP, 0, 0, 1
    )
    routed_in, routed_grad = in_one_piece((part_in, part_grad), "tp", 3, 0)
    gate_pre = jnp.einsum(
        "secd,edf->secf", routed_in, gate_weight, preferred_element_type=jnp.float32
    )
    up_pre = jnp.einsum("secd,edf->secf", routed_in, up_weight, preferred_element_type=jnp.float32)
    sigmoid_gate = jax.nn.sigmoid(gate_pre)
    active = gate_pre * sigmoid_gate
    hidden = (active * up_pre).astype(jnp.bfloat16)
    hidden_grad = jnp.einsum(
        "secd,efd->secf", routed_grad, down_weight, preferred_element_type=jnp.float32
    )
    gate_grad = (
        hidden_grad * up_pre * sigmoid_gate * (1.0 + gate_pre * (1.0 - sigmoid_gate))
    ).astype(jnp.bfloat16)
    up_grad = (hidden_grad * active).astype(jnp.bfloat16)
    slot_terms = jnp.einsum(
        "secf,edf->secd", gate_grad, gate_weight, preferred_element_type=jnp.float32
    )
    slot_terms = slot_terms + jnp.einsum(
        "secf,edf->secd", up_grad, up_weight, preferred_element_type=jnp.float32
    )
    summed = sum_at_owner(slot_terms.astype(jnp.bfloat16), "tp", 3).astype(jnp.bfloat16)
    returned = lax.all_to_all(summed, SP, split_axis=0, concat_axis=0, tiled=True)
    down_weight_gradient = jnp.einsum(
        "secf,secd->efd", hidden, routed_grad, preferred_element_type=jnp.float32
    ).astype(jnp.bfloat16)
    gate_weight_gradient = jnp.einsum(
        "secd,secf->edf", routed_in, gate_grad, preferred_element_type=jnp.float32
    ).astype(jnp.bfloat16)
    up_weight_gradient = jnp.einsum(
        "secd,secf->edf", routed_in, up_grad, preferred_element_type=jnp.float32
    ).astype(jnp.bfloat16)
    back_rows = returned.reshape(expert_list * expert_capacity, returned.shape[3])
    moe_grad = jnp.sum(
        back_rows[place_into_slots].astype(jnp.float32).reshape(tok_rows, chosen_count, -1), axis=1
    )
    mixer_cols = (cotangent.astype(jnp.float32) + moe_grad).astype(jnp.bfloat16)
    mixer_rows = gathered_copies(mixer_cols, "tp", 1)
    inner_x32 = inner_x.astype(jnp.float32)
    inner_b32 = inner_b.astype(jnp.float32)

    def local_states(x_in, b_in, raw_in):
        x_act, b_blocks, decay_log, scaled = prepare(x_in, b_in, raw_in, decay_rate)
        totals = jnp.exp(jnp.sum(decay_log, axis=(0, 1)))
        initial = jnp.zeros((decay_log.shape[2], decay_log.shape[3], HEAD_DIM, STATE), jnp.float32)
        return (totals, lax.scan(advance, initial, (scaled, decay_log, b_blocks))[0])

    (totals, fresh), states_pull = jax.vjp(local_states, inner_x32, inner_b32, step_raw)
    identity = (jnp.ones_like(totals), jnp.zeros_like(fresh))
    carry_in = prefix_by_axis((totals, fresh), SP, carry_forward, identity)[1]
    output_fn = partial(
        mixer_output, decays=decay_rate, skip_weight=skip_weight, norm_gain=norm_gain
    )
    normed, output_pull = jax.vjp(
        output_fn,
        inner_x32,
        inner_b32,
        inner_c.astype(jnp.float32),
        gate_z.astype(jnp.float32),
        step_raw,
        carry_in,
    )
    norm_rows = normed.astype(jnp.bfloat16)
    grad_out = own_rows(
        lax.dot_general(
            mixer_rows, norm_rows, (((0,), (0,)), ((), ())), preferred_element_type=jnp.float32
        ),
        SP,
    )
    norm_grad = jnp.dot(mixer_rows, w_out, preferred_element_type=jnp.float32)
    x_grad_out, b_grad_out, c_grad, z_grad, raw_grad_out, state_grad = output_pull(norm_grad)
    after_grad = carried_in((totals, state_grad), SP, carry_back, identity)[1]
    x_grad_state, b_grad_state, raw_grad_state = states_pull(
        (jnp.sum(after_grad * carry_in, axis=(2, 3)), after_grad)
    )
    grad_inner_x = (x_grad_out + x_grad_state).astype(jnp.bfloat16)
    grad_inner_b = b_grad_out + b_grad_state
    grad_step_raw = raw_grad_out + raw_grad_state
    return (
        gate_weight_gradient,
        up_weight_gradient,
        down_weight_gradient,
        grad_out,
        grad_inner_x,
        grad_inner_b,
        c_grad,
        z_grad.astype(jnp.bfloat16),
        grad_step_raw,
    )


def solution(mesh):
    finer = Mesh(mesh.devices.reshape(8, 4, 2, mesh.shape["tp"]), ("sp_0", "sp_1", "sp_2", "tp"))
    return jax.shard_map(
        body,
        mesh=finer,
        in_specs=(
            P(SP, "tp"),
            P(SP, "tp"),
            P(SP, None),
            P(SP, None),
            P(SP, None, "tp"),
            P(SP, None, "tp"),
            P(SP, "tp", None),
            P(SP, "tp"),
            P(SP, "tp"),
            P(SP, "tp"),
            P(SP, "tp"),
            P(SP, "tp"),
            P("tp"),
            P("tp"),
            P("tp"),
            P(None, "tp"),
        ),
        out_specs=(
            P(SP, None, "tp"),
            P(SP, None, "tp"),
            P(SP, "tp", None),
            P(SP, "tp"),
            P(SP, "tp"),
            P(SP, "tp"),
            P(SP, "tp"),
            P(SP, "tp"),
            P(SP, "tp"),
        ),
        check_vma=False,
    )
```

profile of v0, /device:TPU:1, one launch (start us, length us, event | category | flops | bytes accessed | tf_op | source)
XLA Modules:
  0.0 419.9 jit_solution(6886294324005378016)
XLA Ops:
  21.1 41.1 %all_to_all.20 = bf16[64,2,8,512]{3,2,1,0:T(8,128)(2,1)S(1)} all-to-all(bf16[64,2,8,512]{3,2,1,0:T(8,128)(2,1)S(1)} %pad_maximum_fusion), channel_id=1, replica_groups=mesh['sp_0'=8,'sp_1'=4,'sp_2'=2,'tp'=4] {'sp_0','sp_1','sp_2'}, dimensions={0} | all-to-all | bytes 2097152 | tf_op jit(solution)/shard_map/all_to_all | solution.py:21
  65.1 3.3 all-reduce.6
  68.5 7.6 %all_gather.53 = bf16[4,1,16]{2,1,0:T(2,128)(2,1)S(1)} all-gather(bf16[1,1,16]{2,1,0:T(2,128)(2,1)S(1)} %convert_bitcast_fusion.44), channel_id=1, replica_groups=mesh['sp_0'=8,'sp_1'=4,'sp_2'=2,'tp'=4] {'sp_1'}, dimensions={0}, use_global_device_ids=true | all-gather | bytes 160 | tf_op jit(solution)/shard_map/all_gather | solution.py:79
  77.3 4.2 all-gather.1
  82.3 28.8 %all-gather.7.cloned.1.call-done = bf16[128,1,8,2048]{3,2,0,1:T(8,128)(2,1)} async-done(((bf16[128,1,8,512]{3,2,0,1:T(8,128)(2,1)}), bf16[128,1,8,2048]{3,2,0,1:T(8,128)(2,1)}) %all-gather.7.cloned.1.call-update) | async-done | bytes 4194320 | tf_op jit(solution)/shard_map/all_gather | solution.py:33
  120.5 4.5 %all-to-all-start.1 = ((bf16[4,64,1,8,512]{4,3,1,2,0:T(8,128)(2,1)}), bf16[4,64,1,8,512]{4,3,1,2,0:T(8,128)(2,1)}, u32[]{:S(2)}, u32[]{:S(2)}) async-start(bf16[4,64,1,8,512]{4,3,1,2,0:T(8,128)(2,1)} %bitcast.960), calls=%async_computation.1 | async-start | bytes 4194304 | tf_op jit(solution)/shard_map/all_to_all | solution.py:47
  126.1 13.7 %all_gather.57 = bf16[4,1,16,64,64]{4,3,2,1,0:T(8,128)(2,1)S(1)} all-gather(bf16[1,1,16,64,64]{4,3,2,1,0:T(8,128)(2,1)S(1)} %fusion.251), channel_id=1, replica_groups=mesh['sp_0'=8,'sp_1'=4,'sp_2'=2,'tp'=4] {'sp_1'}, dimensions={0}, use_global_device_ids=true | all-gather | bytes 655360 | tf_op jit(solution)/shard_map/all_gather | solution.py:79
  142.9 7.7 %all-to-all-done.1 = bf16[4,64,1,8,512]{4,3,1,2,0:T(8,128)(2,1)} async-done(((bf16[4,64,1,8,512]{4,3,1,2,0:T(8,128)(2,1)}), bf16[4,64,1,8,512]{4,3,1,2,0:T(8,128)(2,1)}, u32[]{:S(2)}, u32[]{:S(2)}) %all-to-all-start.1) | async-done | bytes 2097184 | tf_op jit(solution)/shard_map/all_to_all | solution.py:47
  153.4 11.7 %all-to-all-start.2 = ((bf16[64,1,8,512]{3,2,1,0:T(8,128)(2,1)}), bf16[64,1,8,512]{3,2,1,0:T(8,128)(2,1)S(1)}, u32[]{:S(2)}, u32[]{:S(2)}) async-start(bf16[64,1,8,512]{3,2,1,0:T(8,128)(2,1)} %bitcast.45), calls=%async_computation.2 | async-start | bytes 1048576 | tf_op jit(solution)/shard_map/all_to_all | solution.py:259
  167.3 25.6 %all_gather.54 = bf16[8,1,16]{2,1,0:T(2,128)(2,1)S(1)} all-gather(bf16[1,1,16]{2,1,0:T(2,128)(2,1)S(1)} %get-tuple-element.407), channel_id=1, replica_groups=mesh['sp_0'=8,'sp_1'=4,'sp_2'=2,'tp'=4] {'sp_0'}, dimensions={0}, use_global_device_ids=true | all-gather | bytes 288 | tf_op jit(solution)/shard_map/all_gather | solution.py:79
  197.9 3.5 all-to-all-start.3
  201.5 3.0 convolution_bitcast_fusion.7
  208.3 3.5 multiply_reduce_fusion.8
  214.9 5.4 %all-gather.2 = bf16[32,64,64]{2,1,0:T(8,128)(2,1)S(1)} all-gather(bf16[16,64,64]{2,1,0:T(8,128)(2,1)S(1)} %fusion.15), channel_id=4, replica_groups=mesh['sp_0'=8,'sp_1'=4,'sp_2'=2,'tp'=4] {'sp_2'}, dimensions={0}, use_global_device_ids=true | all-gather | bytes 393216 | tf_op jit(solution)/shard_map/all_gather | solution.py:106
  220.5 13.2 %all_gather.61 = bf16[4,1,16,64,64]{4,3,2,1,0:T(8,128)(2,1)S(1)} all-gather(bf16[1,1,16,64,64]{4,3,2,1,0:T(8,128)(2,1)S(1)} %fusion.257), channel_id=1, replica_groups=mesh['sp_0'=8,'sp_1'=4,'sp_2'=2,'tp'=4] {'sp_1'}, dimensions={0}, use_global_device_ids=true | all-gather | bytes 655360 | tf_op jit(solution)/shard_map/all_gather | solution.py:106
  235.0 5.8 %fusion.261 = f32[2048,1024]{1,0:T(8,128)} fusion(bf16[128,2048]{0,1:T(8,128)(2,1)} %bitcast.967, f32[128,1024]{1,0:T(8,128)} %copy-done.13, f32[1024]{0:T(1024)S(1)} %copy-done.68, f32[128]{0:T(128)S(1)} %copy-done.59), kind=kOutput, calls=%fused_computation.373 | convolution fusion | flops 537264128 | bytes 9441792 | tf_op jit(solution)/shard_map/dot_general | solution.py:301
  245.0 12.0 %all_gather.63 = bf16[8,1,16]{2,1,0:T(2,128)(2,1)S(1)} all-gather(bf16[1,1,16]{2,1,0:T(2,128)(2,1)S(1)} %copy-done.81), channel_id=1, replica_groups=mesh['sp_0'=8,'sp_1'=4,'sp_2'=2,'tp'=4] {'sp_0'}, dimensions={0}, use_global_device_ids=true | all-gather | bytes 288 | tf_op jit(solution)/shard_map/all_gather | solution.py:106
  260.0 3.7 fusion.4
  278.7 3.2 convolution_bitcast_fusion.10
  282.7 3.3 fusion.71
  291.4 79.3 %reduce-scatter.4.cloned.1.call-done = f32[256,1024]{1,0:T(8,128)} async-done(((f32[2048,1024]{1,0:T(8,128)}), f32[256,1024]{1,0:T(8,128)}) %reduce-scatter.4.cloned.1.call-update) | async-done | bytes 1048592 | tf_op jit(solution)/shard_map/reduce_scatter | solution.py:96
  371.1 5.8 %multiply_reduce_fusion.4 = (f32[16]{0:T(128)}, f32[16]{0:T(128)S(1)}, f32[16]{0:T(128)}) fusion(pred[]{:T(512)S(6)} %lt.80, pred[]{:T(512)S(6)} %lt.79, pred[]{:T(512)S(6)} %lt.78, pred[]{:T(512)S(6)} %lt.77, pred[]{:T(512)S(6)} %lt.76, pred[]{:T(512)S(6)} %lt.75, pred[]{:T(512)S(6)} %lt.74, f32[16]{0:T(128)} %fusion.411, ...), kind=kLoop, calls=%fused_computation.321 | loop fusion | flops 7864272 | bytes 3672156 | tf_op jit(solution)/shard_map/reduce_sum | solution.py:310
  385.9 8.5 %reduce-scatter.6.cloned.1.call-done = f32[64,1024]{1,0:T(8,128)} async-done(((f32[256,1024]{1,0:T(8,128)}), f32[64,1024]{1,0:T(8,128)}) %reduce-scatter.6.cloned.1.call-update) | async-done | bytes 262160 | tf_op jit(solution)/shard_map/reduce_scatter | solution.py:96
  397.6 15.0 %reduce-scatter.8.cloned.1.call-done = f32[32,1024]{1,0:T(8,128)} async-done(((f32[64,1024]{1,0:T(8,128)}), f32[32,1024]{1,0:T(8,128)}) %reduce-scatter.8.cloned.1.call-update) | async-done | bytes 131088 | tf_op jit(solution)/shard_map/reduce_scatter | solution.py:96
  (326 shorter events, 89.3 us)
Async XLA Ops:
  8.0 103.0 %copy-start = (bf16[1,2048,256]{2,1,0:T(8,128)(2,1)S(1)}, bf16[1,2048,256]{2,1,0:T(8,128)(2,1)}, u32[]{:S(2)}) copy-start(bf16[1,2048,256]{2,1,0:T(8,128)(2,1)} %param.21) | copy-start | bytes 3145732
  8.0 103.0 %all-gather.7.cloned.1.call-start = ((), (), s32[]{:S(2)}) async-start(), calls=%async_computation.7 | async-start | bytes 5242880 | tf_op jit(solution)/shard_map/all_gather | solution.py:33
  68.4 56.6 %copy-start.42 = (bf16[32]{0:T(256)(128)(2,1)}, bf16[32]{0:T(256)(128)(2,1)S(1)}, u32[]{:S(2)}) copy-start(bf16[32]{0:T(256)(128)(2,1)S(1)} %all-reduce.6) | copy-start | bytes 196
  76.1 63.7 %copy-start.32 = (bf16[4,1,16]{2,1,0:T(2,128)(2,1)}, bf16[4,1,16]{2,1,0:T(2,128)(2,1)S(1)}, u32[]{:S(2)}) copy-start(bf16[4,1,16]{2,1,0:T(2,128)(2,1)S(1)} %all_gather.53) | copy-start | bytes 388
  81.5 119.9 %copy-start.2 = (bf16[32,64,64]{2,1,0:T(8,128)(2,1)}, bf16[32,64,64]{2,1,0:T(8,128)(2,1)S(1)}, u32[]{:S(2)}) copy-start(bf16[32,64,64]{2,1,0:T(8,128)(2,1)S(1)} %all-gather.1) | copy-start | bytes 786436
  82.3 43.3 %copy-start.64 = (f32[16]{0:T(128)}, f32[16]{0:T(128)S(1)}, u32[]{:S(2)}) copy-start(f32[16]{0:T(128)S(1)} %get-tuple-element.409) | copy-start | bytes 196
  82.3 58.1 %copy-start.60 = (f32[16]{0:T(128)}, f32[16]{0:T(128)S(1)}, u32[]{:S(2)}) copy-start(f32[16]{0:T(128)S(1)} %get-tuple-element.403) | copy-start | bytes 196
  120.5 30.1 %all-to-all-start.1 = ((bf16[4,64,1,8,512]{4,3,1,2,0:T(8,128)(2,1)}), bf16[4,64,1,8,512]{4,3,1,2,0:T(8,128)(2,1)}, u32[]{:S(2)}, u32[]{:S(2)}) async-start(bf16[4,64,1,8,512]{4,3,1,2,0:T(8,128)(2,1)} %bitcast.960), calls=%async_computation.1 | async-start | bytes 4194304 | tf_op jit(solution)/shard_map/all_to_all | solution.py:47
  124.9 76.5 %all-gather.9.cloned.1.call-start = ((), (), s32[]{:S(2)}) async-start(), calls=%async_computation.8 | async-start | bytes 2359296 | tf_op jit(solution)/shard_map/all_gather | solution.py:79
  141.4 23.7 %copy-start.44 = (bf16[128,64]{0,1:T(8,128)(2,1)S(1)}, bf16[128,64]{0,1:T(8,128)(2,1)}, u32[]{:S(2)}) copy-start(bf16[128,64]{0,1:T(8,128)(2,1)} %param.26) | copy-start | bytes 49156
  142.2 24.6 %copy-start.33 = (bf16[4,1,16]{2,1,0:T(2,128)(2,1)S(1)}, bf16[4,1,16]{2,1,0:T(2,128)(2,1)}, u32[]{:S(2)}) copy-start(bf16[4,1,16]{2,1,0:T(2,128)(2,1)} %copy-done.32) | copy-start | bytes 388
  142.2 50.7 %copy-start.70 = (s32[256,1]{0,1:T(1,128)S(1)}, s32[256,1]{0,1:T(1,128)}, u32[]{:S(2)}) copy-start(s32[256,1]{0,1:T(1,128)} %copy-done.69) | copy-start | bytes 3076
  153.4 41.3 %all-to-all-start.2 = ((bf16[64,1,8,512]{3,2,1,0:T(8,128)(2,1)}), bf16[64,1,8,512]{3,2,1,0:T(8,128)(2,1)S(1)}, u32[]{:S(2)}, u32[]{:S(2)}) async-start(bf16[64,1,8,512]{3,2,1,0:T(8,128)(2,1)} %bitcast.45), calls=%async_computation.2 | async-start | bytes 1048576 | tf_op jit(solution)/shard_map/all_to_all | solution.py:259
  165.4 31.5 %copy-start.18 = (bf16[128,512]{1,0:T(8,128)(2,1)S(1)}, bf16[128,512]{1,0:T(8,128)(2,1)}, u32[]{:S(2)}) copy-start(bf16[128,512]{1,0:T(8,128)(2,1)} %param.18) | copy-start | bytes 393220
  197.9 10.4 %all-to-all-start.3 = ((bf16[4,128,512]{1,2,0:T(8,128)(2,1)}), bf16[4,128,512]{1,2,0:T(8,128)(2,1)S(1)}, u32[]{:S(2)}, u32[]{:S(2)}) async-start(bf16[4,128,512]{1,2,0:T(8,128)(2,1)} %broadcast_in_dim.198), calls=%async_computation.3 | async-start | bytes 1048576 | tf_op jit(solution)/shard_map/all_to_all | solution.py:53
  201.3 81.4 %all-gather.11.cloned.1.call-start = ((), (), s32[]{:S(2)}) async-start(), calls=%async_computation.12 | async-start | bytes 2359296 | tf_op jit(solution)/shard_map/all_gather | solution.py:106
  213.3 20.5 %copy-start.49 = (f32[16]{0:T(128)S(1)}, f32[16]{0:T(128)}, u32[]{:S(2)}) copy-start(f32[16]{0:T(128)} %copy-done.48) | copy-start | bytes 196
  213.3 20.4 %copy-start.51 = (f32[16]{0:T(128)S(1)}, f32[16]{0:T(128)}, u32[]{:S(2)}) copy-start(f32[16]{0:T(128)} %copy-done.50) | copy-start | bytes 196
  213.4 20.4 %copy-start.52 = (f32[16]{0:T(128)S(1)}, f32[16]{0:T(128)}, u32[]{:S(2)}) copy-start(f32[16]{0:T(128)} %get-tuple-element.402) | copy-start | bytes 196
  213.4 20.4 %copy-start.53 = (f32[16]{0:T(128)S(1)}, f32[16]{0:T(128)}, u32[]{:S(2)}) copy-start(f32[16]{0:T(128)} %get-tuple-element.398) | copy-start | bytes 196
  234.9 135.8 %reduce-scatter.4.cloned.1.call-start = ((), (), s32[]{:S(2)}) async-start(), calls=%async_computation.9 | async-start | bytes 9437184 | tf_op jit(solution)/shard_map/reduce_scatter | solution.py:96
  240.8 153.6 %reduce-scatter.6.cloned.1.call-start = ((), (), s32[]{:S(2)}) async-start(), calls=%async_computation.10 | async-start | bytes 1310720 | tf_op jit(solution)/shard_map/reduce_scatter | solution.py:96
  370.7 41.9 %reduce-scatter.8.cloned.1.call-start = ((), (), s32[]{:S(2)}) async-start(), calls=%async_computation.11 | async-start | bytes 393216 | tf_op jit(solution)/shard_map/reduce_scatter | solution.py:96
  383.8 28.8 %copy-start.1 = (bf16[1,2048,256]{2,1,0:T(8,128)(2,1)S(1)}, bf16[1,2048,256]{2,1,0:T(8,128)(2,1)}, u32[]{:S(2)}) copy-start(bf16[1,2048,256]{2,1,0:T(8,128)(2,1)} %param.21) | copy-start | bytes 3145732
  (80 other events, 577.3 us)
Sparse Core Ops, SparseCore 0:
  63.5 47.4 all-gather.6
  370.8 23.5 reduce-scatter.5
  397.5 15.0 reduce-scatter.7
Sparse Core Ops, SparseCore 1:
  141.5 50.7 all-gather.8
  235.0 35.6 all-gather.10
  273.0 97.6 reduce-scatter.3
where the time goes:
time: 421 us; the launch traced here: 420 us
  waiting for transfers between devices  142 us (34%)
  blocking collectives  126 us (30%)
  matrix products  42.9 us (10%)
  local copies, waits for them, and re-layouts  37.4 us (9%)
  other arithmetic  33.8 us (8%)
  starting transfers between devices  20.2 us (5%)
  between operations  17.4 us (4%)
    reduce_scatter x3, waiting for transfers between devices, own_rows(): subtotal = lax.psum_scatter(subtotal, axis, scatter_dimension=0, tiled=True)  103 us
    all_gather x4, blocking collectives, prefix_by_axis(): lax.all_gather(part.astype(kind), axis)  51.1 us
    all_to_all x1, blocking collectives, sent_together(): lax.all_to_all(both, axis, split_axis=split_dim, concat_axis=concat_dim,...  41.1 us
    all_gather x3, blocking collectives, carried_in(): lax.all_gather(part.astype(kind), axis)  30.6 us
    all_gather x1, waiting for transfers between devices, in_one_piece(): lax.all_gather(both, axis, axis=dim, tiled=True)  28.8 us
    all_to_all x1, starting transfers between devices, body(): lax.all_to_all(summed, SP, split_axis=0, concat_axis=0, tiled=True)  11.7 us
  transfers between devices with their start and end apart: 9, of which 6 were waited for; matrix products, arithmetic and copies ran while one was open for 19% of the time, Pallas kernels for 0%

commit v1 on v0

v1 whole, which is shorter than its diff:
```python
import jax
import jax.numpy as jnp
from jax import lax
from jax.sharding import Mesh
from jax.experimental import pallas as pl
from jax.experimental.pallas import tpu as pltpu
from jax.sharding import PartitionSpec as P

HEAD_DIM = 64
STATE = 64
LANES = 128
SLOTS = 8
EPS = 0.01
SP = ("z", "y", "c")
F32 = jnp.float32
BF16 = jnp.bfloat16
HIGH = lax.Precision.HIGHEST


def shifted(value, step):
    count = lax.axis_size("x")
    return lax.ppermute(value, "x", [(i, (i + step) % count) for i in range(count)])


def to_all(value, axes):
    return lax.all_to_all(value, axes, split_axis=0, concat_axis=0, tiled=True)


def placed(pieces, where):
    out = jnp.zeros((4, *pieces[0].shape), pieces[0].dtype)
    for piece, index in zip(pieces, where):
        out = lax.dynamic_update_index_in_dim(out, piece, index, 0)
    return out


def gathered_x(value):
    mine = lax.axis_index("x")
    half = value.shape[0] // 2
    left, right = shifted(value, 1), shifted(value, -1)
    far = jnp.concatenate([shifted(left[:half], 1), shifted(right[half:], -1)], axis=0)
    return placed(
        (value, left, right, far),
        (mine, (mine + 3) % 4, (mine + 1) % 4, (mine + 2) % 4),
    )


def summed_x(terms):
    mine = lax.axis_index("x")
    half = terms.shape[1] // 2

    def term(offset):
        return lax.dynamic_index_in_dim(terms, (mine + offset) % 4, 0, keepdims=False)

    far = term(2)
    from_left = shifted(far[:half], 1)
    from_right = shifted(far[half:], -1)
    up, down = term(1), term(3)
    up = jnp.concatenate(
        [(up[:half].astype(F32) + from_left.astype(F32)).astype(BF16), up[half:]], axis=0
    )
    down = jnp.concatenate(
        [down[:half], (down[half:].astype(F32) + from_right.astype(F32)).astype(BF16)], axis=0
    )
    low, high = shifted(up, 1), shifted(down, -1)
    return (term(0).astype(F32) + low.astype(F32) + high.astype(F32)).astype(BF16)


def rows_of(tiled):
    cols = tiled.shape[1] // SLOTS
    rows = tiled.reshape(-1, cols, SLOTS, LANES).transpose(0, 2, 1, 3)
    return rows.reshape(-1, cols * LANES)


SMALL, LARGE = 1 << 30, 1 << 32


def softplus(value):
    small = jnp.exp(-jnp.abs(value))
    grown = 1.0 + small
    log_part = jnp.where(
        grown == 1.0, small, jnp.log(grown) * (small / jnp.where(grown == 1.0, 1.0, grown - 1.0))
    )
    return jnp.maximum(value, 0.0) + log_part


def sigmoid(value):
    return 1.0 / (1.0 + jnp.exp(-value))


def mm(left, right):
    return jnp.dot(left.astype(BF16), right.astype(BF16), preferred_element_type=F32)


def mm_nt(left, right):
    return lax.dot_general(
        left.astype(BF16),
        right.astype(BF16),
        (((1,), (1,)), ((), ())),
        preferred_element_type=F32,
    )


def exact(left, right):
    return jnp.dot(left, right, preferred_element_type=F32, precision=HIGH)


def iota(shape, dim):
    return lax.broadcasted_iota(jnp.int32, shape, dim)


def head_lanes(heads, wide):
    return ((iota((heads, wide), 1) >> 6) == iota((heads, wide), 0)).astype(F32)


def head_rows(heads, wide):
    return ((iota((wide, heads), 0) >> 6) == iota((wide, heads), 1)).astype(F32)


def clocks(raw_t, rate):
    step = softplus(raw_t).T
    logs = -step * rate
    tok = logs.shape[0]
    upto = (iota((tok, tok), 0) >= iota((tok, tok), 1)).astype(F32)
    return step, exact(upto, logs)


def routing(ids_t, experts):
    numbers = iota((experts, ids_t.shape[1]), 0)
    first, second = ids_t[0:1, :] == numbers, ids_t[1:2, :] == numbers
    named = jnp.where(first, 1.0, jnp.where(second, 1.0, 0.0))
    tok = ids_t.shape[1]
    earlier = (iota((tok, tok), 0) < iota((tok, tok), 1)).astype(F32)
    before = mm(named, earlier)
    key = jnp.where(named > 0.0, before, -1.0)
    shape = (experts, SLOTS, tok)
    pick = jnp.broadcast_to(key[:, None, :], shape) == iota(shape, 1).astype(F32)
    return first, second, jnp.where(pick, 1.0, 0.0)


def put_tiles(out_ref, rows, experts):
    cols = rows.shape[1] // LANES
    tiled = rows.reshape(experts, SLOTS, rows.shape[1])
    for col in range(cols):
        out_ref[:, col * SLOTS : (col + 1) * SLOTS, :] = tiled[
            :, :, col * LANES : (col + 1) * LANES
        ].astype(BF16)


def put_pieces(out_ref, at, state):
    rows = state.shape[0] // 8
    for col in range(state.shape[1] // LANES):
        piece = state[:, col * LANES : (col + 1) * LANES].reshape(rows, 8, LANES)
        out_ref[col * rows : (col + 1) * rows, at : at + 8, :] = piece.astype(BF16)


def get_pieces(pieces):
    rows = STATE // 8
    cols = pieces.shape[0] // rows
    return jnp.concatenate(
        [pieces[col * rows : (col + 1) * rows].reshape(STATE, LANES) for col in range(cols)],
        axis=1,
    )


def enter_kernel(ids_ref, moe_ref, x_ref, b_ref, raw_ref, rate_ref, out_ref):
    experts = out_ref.shape[0]
    pick = routing(ids_ref[...], experts)[2]
    rows = mm(pick.reshape(experts * SLOTS, -1), moe_ref[...])
    put_tiles(out_ref, rows, experts)
    step, running = clocks(raw_ref[...], rate_ref[...])
    heads, wide = step.shape[1], x_ref.shape[1]
    last = running[-1:, :]
    spread = exact(
        jnp.concatenate(
            [step * jnp.exp(last - running), jnp.broadcast_to(jnp.exp(last), (8, heads))], axis=0
        ),
        head_lanes(heads, wide),
    )
    x = x_ref[...].astype(F32)
    at_end = x * sigmoid(x) * spread[:-8]
    b = b_ref[...].astype(F32)
    put_pieces(out_ref, 32, mm(b * sigmoid(b), at_end))
    total = spread[-8:]
    high = total.astype(BF16).astype(F32)
    mid = (total - high).astype(BF16).astype(F32)
    low = total - high - mid
    row = iota(total.shape, 0)
    tile = jnp.where(row == 0, high, jnp.where(row == 1, mid, jnp.where(row == 2, low, 0.0)))
    rows_at = STATE // 8
    for col in range(wide // LANES):
        part = tile[:, col * LANES : (col + 1) * LANES].astype(BF16)
        out_ref[col * rows_at : (col + 1) * rows_at, 40:48, :] = jnp.broadcast_to(
            part[None], (rows_at, 8, LANES)
        )


def weigh_kernel(ids_ref, weights_ref, cot_ref, out_ref):
    experts = out_ref.shape[0]
    first, second, pick = routing(ids_ref[...], experts)
    weights = weights_ref[...]
    weight_at = jnp.where(first, weights[0:1, :], 0.0) + jnp.where(second, weights[1:2, :], 0.0)
    scaling = jnp.sum(
        pick * jnp.broadcast_to(weight_at[:, None, :], pick.shape), axis=2, keepdims=True
    )
    rows = mm(pick.reshape(experts * SLOTS, -1), cot_ref[...])
    put_tiles(
        out_ref,
        (rows.reshape(experts, SLOTS, -1) * scaling).reshape(experts * SLOTS, -1),
        experts,
    )


def block_decays(got_ref):
    tile = got_ref[:, 40:48, :].astype(F32)
    total = tile[:, 0:1, :] + tile[:, 1:2, :] + tile[:, 2:3, :]
    return jnp.broadcast_to(total, tile.shape)


def ahead_kernel(got_ref, rows_ref, out_ref):
    out_ref[:, :32, :] = rows_ref[...]
    decays = block_decays(got_ref)
    pieces = got_ref[:, 32:40, :].astype(F32)
    total = jnp.zeros(pieces.shape[1:], F32)
    found = []
    for k in range(pieces.shape[0]):
        found.append(total)
        total = total * decays[k] + pieces[k]
    out_ref[:, 32:40, :] = jnp.stack(found, axis=0).astype(BF16)


def behind_kernel(got_ref, pieces_ref, out_ref):
    decays = block_decays(got_ref)
    pieces = pieces_ref[...].astype(F32)
    total = jnp.zeros(pieces.shape[1:], F32)
    found = []
    for k in reversed(range(pieces.shape[0])):
        found.append(total)
        total = total * decays[k] + pieces[k]
    out_ref[...] = jnp.stack(found[::-1], axis=0).astype(BF16)


def combine_kernel(ids_ref, cot_ref, back_ref, out_ref):
    experts = back_ref.shape[0] // SLOTS
    pick = routing(ids_ref[...], experts)[2].reshape(experts * SLOTS, -1)
    moe_grad = mm(pick.T, back_ref[...])
    rows = (cot_ref[...].astype(F32) + moe_grad).astype(BF16)
    for k in range(out_ref.shape[0]):
        out_ref[k] = rows


def halves(value):
    low = iota(value.shape, 1) < HEAD_DIM
    return jnp.where(low, value, 0.0), jnp.where(low, 0.0, value)


def fade_of(column, row, keep):
    return jnp.exp(jnp.where(keep, column - row, -1e30))


def forward_kernel(
    x_ref, z_ref, b_ref, c_ref, raw_ref, rate_ref, skip_ref, gain_ref, got_ref,
    norm_ref, mixed_ref, start_ref, wide_ref,
):
    start = get_pieces(got_ref[:, 32:40, :].astype(F32))
    start_ref[...] = start.astype(BF16)
    step, running = clocks(raw_ref[...], rate_ref[...])
    tok, heads = step.shape
    wide = x_ref.shape[1]
    spread = exact(
        jnp.concatenate(
            [step, jnp.exp(running), jnp.broadcast_to(skip_ref[...], (8, heads))], axis=0
        ),
        head_lanes(heads, wide),
    )
    x = x_ref[...].astype(F32)
    x_act = x * sigmoid(x)
    scaled = x_act * spread[:tok]
    wide_ref[...] = spread[tok : 2 * tok]
    b, c = b_ref[...].astype(F32), c_ref[...].astype(F32)
    b_t, c_t = b * sigmoid(b), c * sigmoid(c)
    c_act = c_t.T
    scores = mm(c_act, b_t)
    mixed = spread[tok : 2 * tok] * mm(c_act, start) + x_act * spread[2 * tok : 2 * tok + 1]
    running_t = running.T
    keep = iota((tok, tok), 0) >= iota((tok, tok), 1)
    for pair in range(heads // 2):
        lanes = slice(pair * LANES, (pair + 1) * LANES)
        mixes = [
            scores * fade_of(running[:, h : h + 1], running_t[h : h + 1, :], keep)
            for h in (2 * pair, 2 * pair + 1)
        ]
        inside = mm(
            jnp.concatenate(mixes, axis=1), jnp.concatenate(halves(scaled[:, lanes]), axis=0)
        )
        mixed_ref[:, lanes] = mixed[:, lanes] + inside
    z = z_ref[...].astype(F32)
    gated = mixed_ref[...] * (z * sigmoid(z))
    scale = lax.rsqrt(jnp.mean(gated * gated, axis=1, keepdims=True) + EPS)
    norm_ref[...] = (gated * scale * gain_ref[...]).astype(BF16)


def gate_back_kernel(
    grad_ref, mixed_ref, z_ref, gain_ref, wide_ref, c_ref, pieces_ref, grad_z_ref, d_mixed_ref
):
    z = z_ref[...].astype(F32)
    sig = sigmoid(z)
    z_act = z * sig
    mixed = mixed_ref[...]
    gated = mixed * z_act
    scale = lax.rsqrt(jnp.mean(gated * gated, axis=1, keepdims=True) + EPS)
    d_norm = grad_ref[...] * gain_ref[...]
    along = jnp.mean(d_norm * gated, axis=1, keepdims=True)
    d_gated = scale * d_norm - gated * (scale * scale * scale * along)
    d_mixed = d_gated * z_act
    c = c_ref[...].astype(F32)
    put_pieces(pieces_ref, 0, mm(c * sigmoid(c), d_mixed * wide_ref[...]))
    d_mixed_ref[...] = d_mixed
    grad_z_ref[...] = (d_gated * mixed * (sig * (1.0 + z * (1.0 - sig)))).astype(BF16)


def inside_back_kernel(
    x_ref, b_ref, c_ref, raw_ref, rate_ref, skip_ref, start_ref, wide_ref, d_mixed_ref,
    grad_x_ref, reach_x_ref, reach_s_ref, at_end_ref, d_b_ref, grad_c_ref, small_ref,
    d_scaled_ref,
):
    step, running = clocks(raw_ref[...], rate_ref[...])
    tok, heads = step.shape
    wide = x_ref.shape[1]
    last = running[-1:, :]
    spread = exact(
        jnp.concatenate(
            [step, jnp.exp(last - running), jnp.broadcast_to(skip_ref[...], (8, heads))], axis=0
        ),
        head_lanes(heads, wide),
    )
    step_wide, end_wide = spread[:tok], spread[tok : 2 * tok]
    x = x_ref[...].astype(F32)
    sig = sigmoid(x)
    x_act = x * sig
    scaled = x_act * step_wide
    d_mixed = d_mixed_ref[...]
    b, c = b_ref[...].astype(F32), c_ref[...].astype(F32)
    sig_c = sigmoid(c)
    b_t, c_t = b * sigmoid(b), c * sig_c
    b_act, c_act = b_t.T, c_t.T
    scores, scores_t = mm(c_act, b_t), mm(b_act, c_t)
    running_t = running.T
    rows, cols = iota((tok, tok), 0), iota((tok, tok), 1)
    keep, keep_t = rows >= cols, rows <= cols
    d_scores = jnp.zeros((tok, tok), F32)
    gained = jnp.zeros((tok, heads), F32)
    lost = jnp.zeros((heads, tok), F32)
    head_at, head_row = iota((tok, heads), 1), iota((heads, tok), 0)
    for pair in range(heads // 2):
        lanes = slice(pair * LANES, (pair + 1) * LANES)
        d_parts = halves(d_mixed[:, lanes])
        mixes_t = []
        for half in (0, 1):
            h = 2 * pair + half
            column, row = running[:, h : h + 1], running_t[h : h + 1, :]
            fade = fade_of(column, row, keep)
            mixes_t.append(scores_t * jnp.exp(jnp.where(keep_t, row - column, -1e30)))
            d_fade = mm_nt(d_parts[half], scaled[:, lanes]) * fade
            d_scores = d_scores + d_fade
            flow = d_fade * scores
            gained = jnp.where(head_at == h, jnp.sum(flow, axis=1, keepdims=True), gained)
            lost = jnp.where(head_row == h, jnp.sum(flow, axis=0, keepdims=True), lost)
        d_scaled_ref[:, lanes] = mm(
            jnp.concatenate(mixes_t, axis=1), jnp.concatenate(d_parts, axis=0)
        )
    start = start_ref[...].astype(F32)
    d_carried = d_mixed * wide_ref[...]
    by_head = head_rows(heads, wide)
    d_scaled = d_scaled_ref[...]
    d_run = gained - lost.T + exact(d_carried * mm(c_act, start), by_head)
    d_step = exact(d_scaled * x_act, by_head)
    small_ref[0] = d_run
    small_ref[1] = d_step
    small_ref[2] = jnp.broadcast_to(jnp.exp(last), (tok, heads))
    d_silu = sig * (1.0 + x * (1.0 - sig))
    grad_x_ref[...] = (d_scaled * step_wide + d_mixed * spread[2 * tok : 2 * tok + 1]) * d_silu
    reach_x_ref[...] = end_wide * step_wide * d_silu
    reach_s_ref[...] = end_wide * x_act
    at_end_ref[...] = (scaled * end_wide).astype(BF16)
    d_b_ref[...] = mm(c_t, d_scores)
    d_c = mm_nt(b_t, d_scores) + mm_nt(start, d_carried)
    grad_c_ref[...] = d_c * (sig_c * (1.0 + c * (1.0 - sig_c)))


def leave_kernel(
    pieces_ref, start_ref, b_ref, raw_ref, rate_ref, base_ref, reach_x_ref, reach_s_ref,
    at_end_ref, d_b_ref, small_ref, grad_x_ref, grad_b_ref, grad_step_ref,
):
    after = get_pieces(pieces_ref[...].astype(F32))
    b = b_ref[...].astype(F32)
    sig_b = sigmoid(b)
    reach = mm((b * sig_b).T, after)
    grad_x_ref[...] = (base_ref[...] + reach * reach_x_ref[...]).astype(BF16)
    tok, wide = reach.shape
    raw = raw_ref[...]
    step = softplus(raw).T
    heads = step.shape[1]
    both = jnp.concatenate(
        [
            reach * reach_s_ref[...],
            jnp.broadcast_to(
                jnp.sum(after * start_ref[...].astype(F32), axis=0, keepdims=True), (8, wide)
            ),
        ],
        axis=0,
    )
    sums = exact(both, head_rows(heads, wide))
    lost = step * sums[:tok]
    d_run = small_ref[0] - lost
    end_part = jnp.sum(lost, axis=0, keepdims=True) + small_ref[2][:1] * sums[tok : tok + 1]
    onward = (iota((tok, tok), 0) <= iota((tok, tok), 1)).astype(F32)
    d_log = exact(onward, d_run) + end_part
    d_step = small_ref[1] + sums[:tok] - d_log * rate_ref[...]
    grad_step_ref[...] = d_step.T * sigmoid(raw)
    d_b = d_b_ref[...] + mm_nt(after, at_end_ref[...])
    grad_b_ref[...] = d_b * (sig_b * (1.0 + b * (1.0 - sig_b)))


def local(kernel, name, outs, args, flops, scratch=()):
    return pl.pallas_call(
        kernel,
        out_shape=outs,
        name=name,
        scratch_shapes=scratch,
        cost_estimate=pl.CostEstimate(flops=flops, bytes_accessed=1 << 21, transcendentals=1 << 18),
    )(*args)


def body(
    moe_input,
    cotangent,
    expert_ids,
    routing_weights,
    gate_weight,
    up_weight,
    down_weight,
    inner_x,
    inner_b,
    inner_c,
    gate_z,
    step_raw,
    decay_rate,
    skip_weight,
    norm_gain,
    w_out,
):
    tok = expert_ids.shape[0]
    heads = decay_rate.shape[0]
    experts = lax.axis_size(SP)
    wide = inner_x.shape[1]
    gate_w, up_w, down_w = gate_weight[0], up_weight[0], down_weight[0]
    ids_t, b_t, c_t, raw_t = expert_ids.T, inner_b.T, inner_c.T, step_raw.T
    rate, skip, gain = decay_rate[None, :], skip_weight[None, :], norm_gain[None, :]
    shape = jax.ShapeDtypeStruct

    sent = local(
        enter_kernel,
        "enter",
        shape((experts, 48, LANES), BF16),
        (ids_t, moe_input, inner_x, b_t, raw_t, rate),
        SMALL,
    )
    got_in = to_all(sent, SP)
    weighed = local(
        weigh_kernel,
        "weigh",
        shape((experts, 32, LANES), BF16),
        (ids_t, routing_weights.T, cotangent),
        SMALL,
    )
    sent = local(
        ahead_kernel, "ahead", shape((experts, 40, LANES), BF16), (got_in, weighed), SMALL
    )
    all_in = gathered_x(rows_of(got_in[:, :32]))
    got = to_all(sent, SP)
    all_grad = gathered_x(rows_of(got[:, :32]))

    norm_rows, mixed, start_state, start_wide = local(
        forward_kernel,
        "forward",
        (
            shape((tok, wide), BF16),
            shape((tok, wide), F32),
            shape((STATE, wide), BF16),
            shape((tok, wide), F32),
        ),
        (inner_x, gate_z, b_t, c_t, raw_t, rate, skip, gain, got),
        LARGE,
    )
    norm_y = to_all(jnp.broadcast_to(norm_rows[None], (4, tok, wide)), "y")
    other = lax.ppermute(norm_y, "c", [(0, 1), (1, 0)])
    core = lax.axis_index("c") == 0
    norm_all = jnp.stack([jnp.where(core, norm_y, other), jnp.where(core, other, norm_y)], axis=1)

    gate_w4 = gate_w.reshape(4, -1, gate_w.shape[1])
    up_w4 = up_w.reshape(4, -1, up_w.shape[1])
    gate_pre = jnp.einsum("krd,kdf->rf", all_in, gate_w4, preferred_element_type=F32)
    up_pre = jnp.einsum("krd,kdf->rf", all_in, up_w4, preferred_element_type=F32)
    down_w4 = down_w.reshape(down_w.shape[0], 4, -1)
    hidden_grad = jnp.einsum("krd,fkd->rf", all_grad, down_w4, preferred_element_type=F32)
    sig_gate = jax.nn.sigmoid(gate_pre)
    active = gate_pre * sig_gate
    hidden = (active * up_pre).astype(BF16)
    gate_grad = (hidden_grad * up_pre * sig_gate * (1.0 + gate_pre * (1.0 - sig_gate))).astype(BF16)
    up_grad = (hidden_grad * active).astype(BF16)
    terms = jnp.einsum("rf,kdf->krd", gate_grad, gate_w4, preferred_element_type=F32)
    terms = terms + jnp.einsum("rf,kdf->krd", up_grad, up_w4, preferred_element_type=F32)
    slot_grad = summed_x(terms.astype(BF16))
    back = to_all(slot_grad.reshape(experts, SLOTS, -1), SP).reshape(experts * SLOTS, -1)
    gate_out = jnp.einsum("krd,rf->kdf", all_in, gate_grad, preferred_element_type=F32)
    up_out = jnp.einsum("krd,rf->kdf", all_in, up_grad, preferred_element_type=F32)
    down_out = jnp.einsum("rf,krd->fkd", hidden, all_grad, preferred_element_type=F32)

    mixer_cols = local(
        combine_kernel,
        "combine",
        shape((4, *cotangent.shape), BF16),
        (ids_t, cotangent, back),
        SMALL,
    )
    mixer4 = to_all(mixer_cols, "x")
    w_out4 = w_out.reshape(4, -1, wide)
    norm_grad = jnp.einsum("ktd,kdn->tn", mixer4, w_out4, preferred_element_type=F32)

    mixer_t = mixer4.transpose(0, 2, 1).reshape(8, 8, 32, tok).transpose(1, 0, 2, 3)
    mixer_t = to_all(mixer_t, ("y", "c"))

    pieces, grad_z, d_mixed = local(
        gate_back_kernel,
        "gate_back",
        (
            shape((experts, 8, LANES), BF16),
            shape((tok, wide), BF16),
            shape((tok, wide), F32),
        ),
        (norm_grad, mixed, gate_z, gain, start_wide, c_t),
        SMALL,
    )
    pieces = to_all(pieces, SP)
    partial = jnp.einsum(
        "kzrt,ktn->zrn",
        mixer_t,
        norm_all.reshape(8, tok, wide),
        preferred_element_type=F32,
    ).astype(BF16)
    grad_out = jnp.sum(to_all(partial, "z").astype(F32), axis=0)
    pieces = local(
        behind_kernel, "behind", shape((experts, 8, LANES), BF16), (got_in, pieces), SMALL
    )
    pieces = to_all(pieces, SP)
    grad_x, reach_x, reach_s, at_end, d_b, grad_c, small = local(
        inside_back_kernel,
        "inside_back",
        (
            shape((tok, wide), F32),
            shape((tok, wide), F32),
            shape((tok, wide), F32),
            shape((tok, wide), BF16),
            shape((STATE, tok), F32),
            shape((STATE, tok), F32),
            shape((3, tok, heads), F32),
        ),
        (inner_x, b_t, c_t, raw_t, rate, skip, start_state, start_wide, d_mixed),
        LARGE,
        (pltpu.VMEM((tok, wide), F32),),
    )
    grad_x, grad_b, grad_step = local(
        leave_kernel,
        "leave",
        (shape((tok, wide), BF16), shape((STATE, tok), F32), shape((heads, tok), F32)),
        (pieces, start_state, b_t, raw_t, rate, grad_x, reach_x, reach_s, at_end, d_b, small),
        SMALL,
    )
    return (
        gate_out.reshape(gate_weight.shape).astype(BF16),
        up_out.reshape(up_weight.shape).astype(BF16),
        down_out.reshape(down_weight.shape).astype(BF16),
        grad_out,
        grad_x,
        grad_b.T,
        grad_c.T,
        grad_z,
        grad_step.T,
    )


def solution(mesh):
    finer = Mesh(mesh.devices.reshape(8, 4, 2, mesh.shape["tp"]), ("z", "y", "c", "x"))
    return jax.shard_map(
        body,
        mesh=finer,
        in_specs=(
            P(SP, "x"),
            P(SP, "x"),
            P(SP, None),
            P(SP, None),
            P(SP, None, "x"),
            P(SP, None, "x"),
            P(SP, "x", None),
            P(SP, "x"),
            P(SP, "x"),
            P(SP, "x"),
            P(SP, "x"),
            P(SP, "x"),
            P("x"),
            P("x"),
            P("x"),
            P(None, "x"),
        ),
        out_specs=(
            P(SP, None, "x"),
            P(SP, None, "x"),
            P(SP, "x", None),
            P(SP, "x"),
            P(SP, "x"),
            P(SP, "x"),
            P(SP, "x"),
            P(SP, "x"),
            P(SP, "x"),
        ),
        check_vma=False,
    )
```

time: 421 us -> 265 us (0.63)
  blocking collectives: 126 us -> 36.1 us
  waiting for transfers between devices: 142 us -> 92.5 us
  starting transfers between devices: 20.2 us -> 62.1 us
  Pallas kernels: 0 us -> 27.7 us
  other arithmetic: 33.8 us -> 8.75 us
  local copies, waits for them, and re-layouts: 37.4 us -> 13.1 us
  matrix products: 42.9 us -> 21.8 us
  between operations: 17.4 us -> 1.14 us
    reduce_scatter x3 -> x0, waiting for transfers between devices: 103 us -> none  [own_rows(): subtotal = lax.psum_scatter(subtotal, axis, scatter_dimension=0, tiled=True)]
    all_gather x7 -> x0, blocking collectives: 81.7 us -> none  [the longest x4 51.1 us: prefix_by_axis(): lax.all_gather(part.astype(kind), axis)]
    all_to_all x3 -> x8, waiting for transfers between devices: 10.4 us -> 55.2 us  [to_all(): return lax.all_to_all(value, axes, split_axis=0, concat_axis=0, tiled=True)]
    ppermute x0 -> x13, waiting for transfers between devices: none -> 37.3 us  [the longest x12 37.3 us: shifted(): lax.ppermute(value, 'x', [(i, (i + step) % count) for i in range(count)])]
    all_gather x3 -> x0, waiting for transfers between devices: 28.8 us -> none  [the longest x1 28.8 us: in_one_piece(): lax.all_gather(both, axis, axis=dim, tiled=True)]
    pallas_call x0 -> x9, Pallas kernels: none -> 27.7 us  [local(): pl.pallas_call(kernel, out_shape=outs, name=name, scratch_shapes=scratch,...]
    all_to_all x3 -> x8, starting transfers between devices: 19.6 us -> 46.1 us  [to_all(): return lax.all_to_all(value, axes, split_axis=0, concat_axis=0, tiled=True)]
    dot_general x24 -> x10, matrix products: 42.9 us -> 21.8 us  [the longest x1 3.7 us: body(): jnp.einsum('ktd,kdn->tn', mixer4, w_out4, preferred_element_type=F32)]
  transfers between devices with their start and end apart: 9 -> 21, of which waited for: 6 -> 16; matrix products, arithmetic and copies ran while one was open for 19% -> 12% of each run, Pallas kernels for 0% -> 9%
where the time goes in v1:
time: 265 us; the launch traced here: 263 us
  waiting for transfers between devices  92.5 us (35%)
  starting transfers between devices  62.1 us (23%)
  blocking collectives  36.1 us (14%)
  Pallas kernels  27.7 us (10%)
  matrix products  21.8 us (8%)
  local copies, waits for them, and re-layouts  13.1 us (5%)
  other arithmetic  8.75 us (3%)
    all_to_all x8, waiting for transfers between devices, to_all(): return lax.all_to_all(value, axes, split_axis=0, concat_axis=0, tiled=True)  55.2 us
    all_to_all x8, starting transfers between devices, to_all(): return lax.all_to_all(value, axes, split_axis=0, concat_axis=0, tiled=True)  46.1 us
    ppermute x12, waiting for transfers between devices, shifted(): lax.ppermute(value, 'x', [(i, (i + step) % count) for i in range(count)])  37.3 us
    all_to_all x1, blocking collectives, to_all(): return lax.all_to_all(value, axes, split_axis=0, concat_axis=0, tiled=True)  36.1 us
    pallas_call x9, Pallas kernels, local(): pl.pallas_call(kernel, out_shape=outs, name=name, scratch_shapes=scratch,...  27.7 us
    ppermute x12, starting transfers between devices, shifted(): lax.ppermute(value, 'x', [(i, (i + step) % count) for i in range(count)])  13.9 us
  transfers between devices with their start and end apart: 21, of which 16 were waited for; matrix products, arithmetic and copies ran while one was open for 12% of the time, Pallas kernels for 9%

profile of v1, /device:TPU:1, one launch (start us, length us, event | category | flops | bytes accessed | tf_op | source)
XLA Modules:
  0.0 263.2 jit_solution(10850013332603654890)
XLA Ops:
  3.9 36.1 %all_to_all.45.got_ref = bf16[64,48,128]{2,1,0:T(8,128)(2,1)S(1)} all-to-all(bf16[64,48,128]{2,1,0:T(8,128)(2,1)} %enter.1), channel_id=1, replica_groups=mesh['z'=8,'y'=4,'c'=2,'x'=4] {'z','y','c'}, dimensions={0} | all-to-all | bytes 1572864 | tf_op jit(solution)/shard_map/all_to_all | solution.py:26
  48.1 6.5 %all-to-all-start.1 = ((bf16[64,40,128]{2,1,0:T(8,128)(2,1)}), bf16[64,40,128]{2,1,0:T(8,128)(2,1)S(1)}, u32[]{:S(2)}, u32[]{:S(2)}) async-start(bf16[64,40,128]{2,1,0:T(8,128)(2,1)} %ahead.1), calls=%async_computation.1 | async-start | bytes 1310720 | tf_op jit(solution)/shard_map/all_to_all | solution.py:26
  59.3 5.8 %collective-permute-done.3 = bf16[256,512]{1,0:T(8,128)(2,1)S(1)} collective-permute-done((bf16[256,512]{1,0:T(8,128)(2,1)S(1)}, bf16[256,512]{1,0:T(8,128)(2,1)S(1)}, u32[]{:S(2)}, u32[]{:S(2)}) %collective-permute-start.3) | collective-permute-done | bytes 262176 | tf_op jit(solution)/shard_map/ppermute | solution.py:22
  70.1 4.8 %all-to-all-done.1.got_ref = bf16[64,40,128]{2,1,0:T(8,128)(2,1)S(1)} async-done(((bf16[64,40,128]{2,1,0:T(8,128)(2,1)}), bf16[64,40,128]{2,1,0:T(8,128)(2,1)S(1)}, u32[]{:S(2)}, u32[]{:S(2)}) %all-to-all-start.1) | async-done | bytes 655392 | tf_op jit(solution)/shard_map/all_to_all | solution.py:26
  80.3 7.9 %collective-permute-done.5 = bf16[512,512]{1,0:T(8,128)(2,1)S(1)} collective-permute-done((bf16[512,512]{1,0:T(8,128)(2,1)S(1)}, bf16[512,512]{1,0:T(8,128)(2,1)S(1)}, u32[]{:S(2)}, u32[]{:S(2)}) %collective-permute-start.5) | collective-permute-done | bytes 524320 | tf_op jit(solution)/shard_map/ppermute | solution.py:22
  92.0 3.6 %collective-permute-done.7 = bf16[256,512]{1,0:T(8,128)(2,1)S(1)} collective-permute-done((bf16[256,512]{1,0:T(8,128)(2,1)S(1)}, bf16[256,512]{1,0:T(8,128)(2,1)S(1)}, u32[]{:S(2)}, u32[]{:S(2)}) %collective-permute-start.7) | collective-permute-done | bytes 262176 | tf_op jit(solution)/shard_map/ppermute | solution.py:22
  104.4 3.6 %collective-permute-done.10 = bf16[256,512]{1,0:T(8,128)(2,1)S(1)} collective-permute-done((bf16[256,512]{1,0:T(8,128)(2,1)S(1)}, bf16[256,512]{1,0:T(8,128)(2,1)S(1)}, u32[]{:S(2)}, u32[]{:S(2)}) %collective-permute-start.10) | collective-permute-done | bytes 262176 | tf_op jit(solution)/shard_map/ppermute | solution.py:22
  111.3 7.4 %collective-permute-done.11 = bf16[512,512]{1,0:T(8,128)(2,1)} collective-permute-done((bf16[512,512]{1,0:T(8,128)(2,1)}, bf16[512,512]{1,0:T(8,128)(2,1)}, u32[]{:S(2)}, u32[]{:S(2)}) %collective-permute-start.11) | collective-permute-done | bytes 524320 | tf_op jit(solution)/shard_map/ppermute | solution.py:22
  124.3 10.8 %all-to-all-start.2 = ((bf16[64,8,512]{2,1,0:T(8,128)(2,1)}), bf16[64,8,512]{2,1,0:T(8,128)(2,1)S(1)}, u32[]{:S(2)}, u32[]{:S(2)}) async-start(bf16[64,8,512]{2,1,0:T(8,128)(2,1)} %fusion.4), calls=%async_computation.2 | async-start | bytes 1048576 | tf_op jit(solution)/shard_map/all_to_all | solution.py:26
  135.1 3.9 %forward.1 = (bf16[128,1024]{1,0:T(8,128)(2,1)}, f32[128,1024]{1,0:T(8,128)}, bf16[64,1024]{1,0:T(8,128)(2,1)}, f32[128,1024]{1,0:T(8,128)}) custom-call(bf16[128,1024]{1,0:T(8,128)(2,1)} %x_ref.5, bf16[128,1024]{1,0:T(8,128)(2,1)} %z_ref.3, bf16[64,128]{1,0:T(8,128)(2,1)} %bitcast.150, bf16[64,128]{1,0:T(8,128)(2,1)} %bitcast.146, f32[16,128]{1,0:T(8,128)} %bitcast.154, ...), custom_call_target="tpu_custom_call" | custom-call | flops 4294967296 | bytes 2097152 | tf_op jit(solution)/shard_map/forward/pallas_call | solution.py:425
  139.0 13.8 %all-to-all-done.2 = bf16[64,8,512]{2,1,0:T(8,128)(2,1)S(1)} async-done(((bf16[64,8,512]{2,1,0:T(8,128)(2,1)}), bf16[64,8,512]{2,1,0:T(8,128)(2,1)S(1)}, u32[]{:S(2)}, u32[]{:S(2)}) %all-to-all-start.2) | async-done | bytes 524320 | tf_op jit(solution)/shard_map/all_to_all | solution.py:26
  155.0 3.5 %all-to-all-start.5 = ((bf16[4,128,1024]{2,1,0:T(8,128)(2,1)}), bf16[4,128,1024]{2,1,0:T(8,128)(2,1)S(1)}, u32[]{:S(2)}, u32[]{:S(2)}) async-start(bf16[4,128,1024]{2,1,0:T(8,128)(2,1)} %broadcast_in_dim.51), calls=%async_computation.5 | async-start | bytes 2097152 | tf_op jit(solution)/shard_map/all_to_all | solution.py:26
  160.9 11.6 %all-to-all-done.5 = bf16[4,128,1024]{2,1,0:T(8,128)(2,1)S(1)} async-done(((bf16[4,128,1024]{2,1,0:T(8,128)(2,1)}), bf16[4,128,1024]{2,1,0:T(8,128)(2,1)S(1)}, u32[]{:S(2)}, u32[]{:S(2)}) %all-to-all-start.5) | async-done | bytes 1048608 | tf_op jit(solution)/shard_map/all_to_all | solution.py:26
  178.1 5.1 %all-to-all-done.3 = bf16[4,128,512]{2,1,0:T(8,128)(2,1)S(1)} async-done(((bf16[4,128,512]{2,1,0:T(8,128)(2,1)}), bf16[4,128,512]{2,1,0:T(8,128)(2,1)S(1)}, u32[]{:S(2)}, u32[]{:S(2)}) %all-to-all-start.3) | async-done | bytes 524320 | tf_op jit(solution)/shard_map/all_to_all | solution.py:26
  183.2 3.7 %convolution_bitcast_fusion.4.grad_ref = f32[128,1024]{1,0:T(8,128)} fusion(bf16[4,128,512]{2,1,0:T(8,128)(2,1)S(1)} %all-to-all-done.3, bf16[4,512,1024]{2,1,0:T(8,128)(2,1)} %bitcast.138), kind=kOutput, calls=%fused_computation.10 | convolution fusion | flops 536870912 | bytes 5242880 | tf_op jit(solution)/shard_map/ktd,kdn->tn/dot_general | solution.py:528
  189.8 8.9 %all-to-all-start.7 = ((bf16[64,8,128]{2,1,0:T(8,128)(2,1)}), bf16[64,8,128]{2,1,0:T(8,128)(2,1)S(1)}, u32[]{:S(2)}, u32[]{:S(2)}) async-start(bf16[64,8,128]{2,1,0:T(8,128)(2,1)} %get-tuple-element.29), calls=%async_computation.7 | async-start | bytes 262144 | tf_op jit(solution)/shard_map/all_to_all | solution.py:26
  203.3 6.4 %all-to-all-done.7.pieces_ref = bf16[64,8,128]{2,1,0:T(8,128)(2,1)S(1)} async-done(((bf16[64,8,128]{2,1,0:T(8,128)(2,1)}), bf16[64,8,128]{2,1,0:T(8,128)(2,1)S(1)}, u32[]{:S(2)}, u32[]{:S(2)}) %all-to-all-start.7) | async-done | bytes 131104 | tf_op jit(solution)/shard_map/all_to_all | solution.py:26
  209.8 3.8 %all-to-all-start.4 = ((bf16[8,8,32,128]{3,2,1,0:T(8,128)(2,1)}), bf16[8,8,32,128]{3,2,1,0:T(8,128)(2,1)S(1)}, u32[]{:S(2)}, u32[]{:S(2)}) async-start(bf16[8,8,32,128]{3,2,1,0:T(8,128)(2,1)} %copy.44), calls=%async_computation.4 | async-start | bytes 1048576 | tf_op jit(solution)/shard_map/all_to_all | solution.py:26
  218.4 4.5 %all-to-all-done.4 = bf16[8,8,32,128]{3,2,1,0:T(8,128)(2,1)S(1)} async-done(((bf16[8,8,32,128]{3,2,1,0:T(8,128)(2,1)}), bf16[8,8,32,128]{3,2,1,0:T(8,128)(2,1)S(1)}, u32[]{:S(2)}, u32[]{:S(2)}) %all-to-all-start.4) | async-done | bytes 524320 | tf_op jit(solution)/shard_map/all_to_all | solution.py:26
  222.9 5.0 %all-to-all-start.8 = ((bf16[64,8,128]{2,1,0:T(8,128)(2,1)}), bf16[64,8,128]{2,1,0:T(8,128)(2,1)S(1)}, u32[]{:S(2)}, u32[]{:S(2)}) async-start(bf16[64,8,128]{2,1,0:T(8,128)(2,1)} %behind.1), calls=%async_computation.8 | async-start | bytes 262144 | tf_op jit(solution)/shard_map/all_to_all | solution.py:26
  231.4 7.9 %all-to-all-done.8.pieces_ref = bf16[64,8,128]{2,1,0:T(8,128)(2,1)S(1)} async-done(((bf16[64,8,128]{2,1,0:T(8,128)(2,1)}), bf16[64,8,128]{2,1,0:T(8,128)(2,1)S(1)}, u32[]{:S(2)}, u32[]{:S(2)}) %all-to-all-start.8) | async-done | bytes 131104 | tf_op jit(solution)/shard_map/all_to_all | solution.py:26
  239.3 4.2 %all-to-all-start.6 = ((bf16[8,32,1024]{2,1,0:T(8,128)(2,1)}), bf16[8,32,1024]{2,1,0:T(8,128)(2,1)}, u32[]{:S(2)}, u32[]{:S(2)}) async-start(bf16[8,32,1024]{2,1,0:T(8,128)(2,1)} %fusion), calls=%async_computation.6 | async-start | bytes 1048576 | tf_op jit(solution)/shard_map/all_to_all | solution.py:26
  251.5 5.3 %inside_back.1 = (f32[128,1024]{1,0:T(8,128)}, f32[128,1024]{1,0:T(8,128)}, f32[128,1024]{1,0:T(8,128)}, bf16[128,1024]{1,0:T(8,128)(2,1)}, f32[64,128]{1,0:T(8,...) custom-call(bf16[128,1024]{1,0:T(8,128)(2,1)} %x_ref.5, bf16[64,128]{1,0:T(8,128)(2,1)} %bitcast.151, ...), custom_call_target="tpu_custom_call" | custom-call | flops 4294967296 | bytes 2097152 | tf_op jit(solution)/shard_map/inside_back/pallas_call | solution.py:425
  256.7 3.6 %leave.1 = (bf16[128,1024]{1,0:T(8,128)(2,1)}, f32[64,128]{1,0:T(8,128)}, f32[16,128]{1,0:T(8,128)}) custom-call(bf16[64,8,128]{2,1,0:T(8,128)(2,1)} %copy-done.14, bf16[64,1024]{1,0:T(8,128)(2,1)} %get-tuple-element.30.start_ref, bf16[64,128]{1,0:T(8,128)(2,1)} %bitcast.152, f32[16,128]{1,0:T(8,128)} %bitcast.156, f32[1,16]{1,0:T(1,128)} %bitcast.168, ...), custom_call_target="tpu_custom_call" | custom-call | flops 1073741824 | bytes 2097152 | tf_op jit(solution)/shard_map/leave/pallas_call | solution.py:425
  (110 shorter events, 84.3 us)
Async XLA Ops:
  0.6 66.6 %copy-start = (bf16[1,2048,256]{2,1,0:T(8,128)(2,1)S(1)}, bf16[1,2048,256]{2,1,0:T(8,128)(2,1)}, u32[]{:S(2)}) copy-start(bf16[1,2048,256]{2,1,0:T(8,128)(2,1)} %param.20) | copy-start | bytes 3145732
  40.9 18.0 %collective-permute-start = (bf16[512,512]{1,0:T(8,128)(2,1)}, bf16[512,512]{1,0:T(8,128)(2,1)S(1)}, u32[]{:S(2)}, u32[]{:S(2)}) collective-permute-start(bf16[512,512]{1,0:T(8,128)(2,1)} %slice_bitcast_fusion.1), channel_id=1, source_target_pairs={{0,1},{1,2},{2,3},{3,0},{4,5},{5,6},{6,7},{7,4},{8,9},{9,10},{10,1... | collective-permute-start | bytes 1572872 | tf_op jit(solution)/shard_map/ppermute | solution.py:22
  42.2 15.4 %collective-permute-start.1 = (bf16[512,512]{1,0:T(8,128)(2,1)}, bf16[512,512]{1,0:T(8,128)(2,1)S(1)}, u32[]{:S(2)}, u32[]{:S(2)}) collective-permute-start(bf16[512,512]{1,0:T(8,128)(2,1)} %slice_bitcast_fusion.1), channel_id=1, source_target_pairs={{0,3},{1,0},{2,1},{3,2},{4,7},{5,4},{6,5},{7,6},{8,11},{9,8},{10,9... | collective-permute-start | bytes 1572872 | tf_op jit(solution)/shard_map/ppermute | solution.py:22
  48.1 26.8 %all-to-all-start.1 = ((bf16[64,40,128]{2,1,0:T(8,128)(2,1)}), bf16[64,40,128]{2,1,0:T(8,128)(2,1)S(1)}, u32[]{:S(2)}, u32[]{:S(2)}) async-start(bf16[64,40,128]{2,1,0:T(8,128)(2,1)} %ahead.1), calls=%async_computation.1 | async-start | bytes 1310720 | tf_op jit(solution)/shard_map/all_to_all | solution.py:26
  57.6 7.5 %collective-permute-start.3 = (bf16[256,512]{1,0:T(8,128)(2,1)S(1)}, bf16[256,512]{1,0:T(8,128)(2,1)S(1)}, u32[]{:S(2)}, u32[]{:S(2)}) collective-permute-start(bf16[256,512]{1,0:T(8,128)(2,1)S(1)} %slice.68), channel_id=1, source_target_pairs={{0,3},{1,0},{2,1},{3,2},{4,7},{5,4},{6,5},{7,6},{8,11},{9,8},{10,9... | collective-permute-start | bytes 786440 | tf_op jit(solution)/shard_map/ppermute | solution.py:22
  58.9 8.3 %collective-permute-start.2 = (bf16[256,512]{1,0:T(8,128)(2,1)S(1)}, bf16[256,512]{1,0:T(8,128)(2,1)S(1)}, u32[]{:S(2)}, u32[]{:S(2)}) collective-permute-start(bf16[256,512]{1,0:T(8,128)(2,1)S(1)} %slice.67), channel_id=1, source_target_pairs={{0,1},{1,2},{2,3},{3,0},{4,5},{5,6},{6,7},{7,4},{8,9},{9,10},{10,1... | collective-permute-start | bytes 786440 | tf_op jit(solution)/shard_map/ppermute | solution.py:22
  74.9 16.7 %collective-permute-start.4 = (bf16[512,512]{1,0:T(8,128)(2,1)S(1)}, bf16[512,512]{1,0:T(8,128)(2,1)S(1)}, u32[]{:S(2)}, u32[]{:S(2)}) collective-permute-start(bf16[512,512]{1,0:T(8,128)(2,1)S(1)} %slice_bitcast_fusion), channel_id=1, source_target_pairs={{0,1},{1,2},{2,3},{3,0},{4,5},{5,6},{6,7},{7,4},{8,9},{9,10},{10,1... | collective-permute-start | bytes 1572872 | tf_op jit(solution)/shard_map/ppermute | solution.py:22
  75.0 13.1 %collective-permute-start.5 = (bf16[512,512]{1,0:T(8,128)(2,1)S(1)}, bf16[512,512]{1,0:T(8,128)(2,1)S(1)}, u32[]{:S(2)}, u32[]{:S(2)}) collective-permute-start(bf16[512,512]{1,0:T(8,128)(2,1)S(1)} %slice_bitcast_fusion), channel_id=1, source_target_pairs={{0,3},{1,0},{2,1},{3,2},{4,7},{5,4},{6,5},{7,6},{8,11},{9,8},{10,9... | collective-permute-start | bytes 1572872 | tf_op jit(solution)/shard_map/ppermute | solution.py:22
  80.0 19.1 %copy-start.18 = (f32[512,256]{1,0:T(8,128)}, f32[512,256]{1,0:T(8,128)S(1)}, u32[]{:S(2)}) copy-start(f32[512,256]{1,0:T(8,128)S(1)} %convolution_bitcast_fusion.2) | copy-start | bytes 1572868
  80.2 18.9 %copy-start.7 = (bf16[256,4,512]{2,1,0:T(4,128)(2,1)S(1)}, bf16[256,4,512]{2,1,0:T(4,128)(2,1)}, u32[]{:S(2)}) copy-start(bf16[256,4,512]{2,1,0:T(4,128)(2,1)} %reshape_squeeze.9) | copy-start | bytes 3145732
  88.2 7.5 %collective-permute-start.7 = (bf16[256,512]{1,0:T(8,128)(2,1)S(1)}, bf16[256,512]{1,0:T(8,128)(2,1)S(1)}, u32[]{:S(2)}, u32[]{:S(2)}) collective-permute-start(bf16[256,512]{1,0:T(8,128)(2,1)S(1)} %slice.71), channel_id=1, source_target_pairs={{0,3},{1,0},{2,1},{3,2},{4,7},{5,4},{6,5},{7,6},{8,11},{9,8},{10,9... | collective-permute-start | bytes 786440 | tf_op jit(solution)/shard_map/ppermute | solution.py:22
  91.7 7.4 %collective-permute-start.6 = (bf16[256,512]{1,0:T(8,128)(2,1)S(1)}, bf16[256,512]{1,0:T(8,128)(2,1)S(1)}, u32[]{:S(2)}, u32[]{:S(2)}) collective-permute-start(bf16[256,512]{1,0:T(8,128)(2,1)S(1)} %slice.70), channel_id=1, source_target_pairs={{0,1},{1,2},{2,3},{3,0},{4,5},{5,6},{6,7},{7,4},{8,9},{9,10},{10,1... | collective-permute-start | bytes 786440 | tf_op jit(solution)/shard_map/ppermute | solution.py:22
  102.7 5.3 %collective-permute-start.10 = (bf16[256,512]{1,0:T(8,128)(2,1)S(1)}, bf16[256,512]{1,0:T(8,128)(2,1)S(1)}, u32[]{:S(2)}, u32[]{:S(2)}) collective-permute-start(bf16[256,512]{1,0:T(8,128)(2,1)S(1)} %get-tuple-element.69), channel_id=1, source_target_pairs={{0,3},{1,0},{2,1},{3,2},{4,7},{5,4},{6,5},{7,6},{8,11},{9,8},{10,9... | collective-permute-start | bytes 786440 | tf_op jit(solution)/shard_map/ppermute | solution.py:22
  102.8 7.3 %collective-permute-start.8 = (bf16[256,512]{1,0:T(8,128)(2,1)S(1)}, bf16[256,512]{1,0:T(8,128)(2,1)S(1)}, u32[]{:S(2)}, u32[]{:S(2)}) collective-permute-start(bf16[256,512]{1,0:T(8,128)(2,1)S(1)} %get-tuple-element.68), channel_id=1, source_target_pairs={{0,1},{1,2},{2,3},{3,0},{4,5},{5,6},{6,7},{7,4},{8,9},{9,10},{10,1... | collective-permute-start | bytes 786440 | tf_op jit(solution)/shard_map/ppermute | solution.py:22
  108.9 9.8 %collective-permute-start.11 = (bf16[512,512]{1,0:T(8,128)(2,1)}, bf16[512,512]{1,0:T(8,128)(2,1)}, u32[]{:S(2)}, u32[]{:S(2)}) collective-permute-start(bf16[512,512]{1,0:T(8,128)(2,1)} %pad_maximum_fusion.2), channel_id=1, source_target_pairs={{0,3},{1,0},{2,1},{3,2},{4,7},{5,4},{6,5},{7,6},{8,11},{9,8},{10,9... | collective-permute-start | bytes 1572872 | tf_op jit(solution)/shard_map/ppermute | solution.py:22
  111.0 11.0 %collective-permute-start.9 = (bf16[512,512]{1,0:T(8,128)(2,1)}, bf16[512,512]{1,0:T(8,128)(2,1)}, u32[]{:S(2)}, u32[]{:S(2)}) collective-permute-start(bf16[512,512]{1,0:T(8,128)(2,1)} %pad_maximum_fusion.1), channel_id=1, source_target_pairs={{0,1},{1,2},{2,3},{3,0},{4,5},{5,6},{6,7},{7,4},{8,9},{9,10},{10,1... | collective-permute-start | bytes 1572872 | tf_op jit(solution)/shard_map/ppermute | solution.py:22
  124.3 28.5 %all-to-all-start.2 = ((bf16[64,8,512]{2,1,0:T(8,128)(2,1)}), bf16[64,8,512]{2,1,0:T(8,128)(2,1)S(1)}, u32[]{:S(2)}, u32[]{:S(2)}) async-start(bf16[64,8,512]{2,1,0:T(8,128)(2,1)} %fusion.4), calls=%async_computation.2 | async-start | bytes 1048576 | tf_op jit(solution)/shard_map/all_to_all | solution.py:26
  155.0 17.5 %all-to-all-start.5 = ((bf16[4,128,1024]{2,1,0:T(8,128)(2,1)}), bf16[4,128,1024]{2,1,0:T(8,128)(2,1)S(1)}, u32[]{:S(2)}, u32[]{:S(2)}) async-start(bf16[4,128,1024]{2,1,0:T(8,128)(2,1)} %broadcast_in_dim.51), calls=%async_computation.5 | async-start | bytes 2097152 | tf_op jit(solution)/shard_map/all_to_all | solution.py:26
  172.5 10.7 %all-to-all-start.3 = ((bf16[4,128,512]{2,1,0:T(8,128)(2,1)}), bf16[4,128,512]{2,1,0:T(8,128)(2,1)S(1)}, u32[]{:S(2)}, u32[]{:S(2)}) async-start(bf16[4,128,512]{2,1,0:T(8,128)(2,1)} %combine.1), calls=%async_computation.3 | async-start | bytes 1048576 | tf_op jit(solution)/shard_map/all_to_all | solution.py:26
  176.0 37.6 %collective-permute-start.12 = (bf16[4,128,1024]{2,1,0:T(8,128)(2,1)S(1)}, bf16[4,128,1024]{2,1,0:T(8,128)(2,1)}, u32[]{:S(2)}, u32[]{:S(2)}) collective-permute-start(bf16[4,128,1024]{2,1,0:T(8,128)(2,1)S(1)} %all-to-all-done.5), channel_id=1, source_target_pairs={{0,4},{4,0},{1,5},{5,1},{2,6},{6,2},{3,7},{7,3},{8,12},{12,8},{9,1... | collective-permute-start | bytes 3145736 | tf_op jit(solution)/shard_map/ppermute | solution.py:496
  189.8 20.0 %all-to-all-start.7 = ((bf16[64,8,128]{2,1,0:T(8,128)(2,1)}), bf16[64,8,128]{2,1,0:T(8,128)(2,1)S(1)}, u32[]{:S(2)}, u32[]{:S(2)}) async-start(bf16[64,8,128]{2,1,0:T(8,128)(2,1)} %get-tuple-element.29), calls=%async_computation.7 | async-start | bytes 262144 | tf_op jit(solution)/shard_map/all_to_all | solution.py:26
  209.8 13.2 %all-to-all-start.4 = ((bf16[8,8,32,128]{3,2,1,0:T(8,128)(2,1)}), bf16[8,8,32,128]{3,2,1,0:T(8,128)(2,1)S(1)}, u32[]{:S(2)}, u32[]{:S(2)}) async-start(bf16[8,8,32,128]{3,2,1,0:T(8,128)(2,1)} %copy.44), calls=%async_computation.4 | async-start | bytes 1048576 | tf_op jit(solution)/shard_map/all_to_all | solution.py:26
  222.9 16.3 %all-to-all-start.8 = ((bf16[64,8,128]{2,1,0:T(8,128)(2,1)}), bf16[64,8,128]{2,1,0:T(8,128)(2,1)S(1)}, u32[]{:S(2)}, u32[]{:S(2)}) async-start(bf16[64,8,128]{2,1,0:T(8,128)(2,1)} %behind.1), calls=%async_computation.8 | async-start | bytes 262144 | tf_op jit(solution)/shard_map/all_to_all | solution.py:26
  239.3 22.1 %all-to-all-start.6 = ((bf16[8,32,1024]{2,1,0:T(8,128)(2,1)}), bf16[8,32,1024]{2,1,0:T(8,128)(2,1)}, u32[]{:S(2)}, u32[]{:S(2)}) async-start(bf16[8,32,1024]{2,1,0:T(8,128)(2,1)} %fusion), calls=%async_computation.6 | async-start | bytes 1048576 | tf_op jit(solution)/shard_map/all_to_all | solution.py:26
  (16 other events, 98.6 us)
